TPU v7x, 512 devices: a whole 4x4x16 slice. The times are simulated.
512 devices in a mesh: sp: 64 (over z, y), dp: 8 (over x, core).
Axes of the slice: x: 4, y: 4, z: 16, core: 2. Of those that a mesh axis runs over, the one named last changes fastest.
Arguments:
- gate_input: bfloat16 [8, 12288, 4096], P('dp', 'sp'), may hold values from -6 to 6
- value_input: bfloat16 [8, 12288, 4096], P('dp', 'sp'), may hold values from -6 to 6
- norm_gain: float32 [4096], replicated, may hold values from 0.1 to 1.9
- norm_bias: float32 [4096], replicated, may hold values from -3 to 3
- mix_weight: bfloat16 [64, 1024, 1024], P('sp', 'dp'), may hold values from -0.1875 to 0.1875
- mix_bias: float32 [64, 1024], P('sp'), may hold values from 0.1 to 1.9
Outputs:
- gated: bfloat16 [8, 12288, 4096], P('dp', 'sp')
All inputs are finite; a program needn't handle non-finite values.
Results may differ from a plain program's by a relative error of at most 0.0053.
Values may be sent and summed in bfloat16 or wider, within the bound.
No kernel may reach another device: no remote copies, remote signals or barrier semaphores. Data moves between devices by JAX's collectives and lax.ppermute only.
A program may use at most 64 MiB of HBM per device.

v0:
```python
import jax
import jax.numpy as jnp
from jax import lax
from jax.sharding import Mesh
from jax.sharding import PartitionSpec as P

GROUP_DIM = 64
SPAN = 1024
DP = ("dp_0", "dp_1")
epsilon = 1e-05


def joined_along(parts, dim):
    parts = jnp.moveaxis(parts, 0, dim)
    lengths = parts.shape
    return parts.reshape(*lengths[:dim], lengths[dim] * lengths[dim + 1], *lengths[dim + 2 :])


def all_blocks(shard, axes, sequence):
    parts = shard[None]
    for k in sequence:
        parts = lax.all_gather(parts, axes[k], axis=0, tiled=True)
    current = [lax.axis_size(axes[k]) for k in reversed(sequence)]
    parts = parts.reshape(*current, *shard.shape)
    turned = sorted(range(len(sequence)), key=lambda place: sequence[len(sequence) - 1 - place])
    return parts.transpose(*turned, *range(len(sequence), parts.ndim)).reshape(-1, *shard.shape)


def gather_axes(shard, axes, sequence, dim):
    return joined_along(all_blocks(shard, axes, sequence), dim)


def local(gate_input, value_input, norm_gain, norm_bias, mix_weight, mix_bias):
    token_rows = value_input.shape[1]
    channels = value_input.shape[2]
    act_value = jax.nn.gelu(value_input[0].astype(jnp.float32))
    centre = jnp.mean(act_value, axis=-1, keepdims=True)
    shifted = act_value - centre
    variance = jnp.mean(shifted * shifted, axis=-1, keepdims=True)
    normed = (shifted * lax.rsqrt(variance + epsilon) * norm_gain + norm_bias).astype(jnp.bfloat16)
    normed_group = lax.all_to_all(normed, "sp", split_axis=1, concat_axis=0, tiled=True)
    positions = normed_group.shape[0]
    group_count = mix_weight.shape[0]
    blocks = normed_group.reshape(positions // SPAN, SPAN, group_count, GROUP_DIM)
    columns = lax.broadcasted_iota(jnp.int32, (1, SPAN), 1)
    weight_rows = gather_axes(mix_weight, DP, (0, 1), 1)
    row_count = weight_rows.shape[1]
    rows_index = lax.broadcasted_iota(jnp.int32, (row_count, 1), 0)
    masked = jnp.where((columns <= rows_index)[None], weight_rows, jnp.zeros_like(weight_rows))
    summed = jnp.einsum("gqp,npgc->nqgc", masked, blocks, preferred_element_type=jnp.float32)
    mixed_blocks = (summed + mix_bias.T[None, :, :, None]).astype(jnp.bfloat16)
    mixed_flat = lax.optimization_barrier(mixed_blocks.reshape(positions, group_count * GROUP_DIM))
    returned = lax.all_to_all(mixed_flat, "sp", split_axis=0, concat_axis=1, tiled=True)
    gated_rows = (
        jax.nn.gelu(gate_input[0].astype(jnp.float32)) * returned.astype(jnp.float32)
    ).astype(jnp.bfloat16)
    return gated_rows.reshape(1, token_rows, channels)


def solution(mesh):
    split = Mesh(mesh.devices.reshape(mesh.shape["sp"], 4, 2), ("sp", "dp_0", "dp_1"))
    in_specs = (P(DP, "sp", None), P(DP, "sp", None), P(), P(), P("sp", DP, None), P("sp", None))
    out_specs = P(DP, "sp", None)
    return jax.shard_map(local, mesh=split, in_specs=in_specs, out_specs=out_specs, check_vma=False)
```

profile of v0, /device:TPU:2, one launch (start us, length us, event | category | flops | bytes accessed | tf_op | source)
XLA Modules:
  0.0 276.7 jit_solution(663343438426462109)
XLA Ops:
  6.5 0.8 mul.82
  7.3 0.8 add.70
  8.1 3.1 %copy.24 = bf16[1,192,4096]{1,2,0:T(8,128)(2,1)S(1)} copy(bf16[1,192,4096]{2,1,0:T(8,128)(2,1)} %param.7) | data formatting | bytes 3145728 | tf_op args[1]
  11.3 1.6 fusion.28
  12.8 1.8 multiply_reduce_fusion
  14.7 3.1 %fusion.18 = bf16[192,64,64]{0,2,1:T(8,128)(2,1)} fusion(f32[64,64]{1,0:T(8,128)S(1)} %add.70, f32[64,64]{1,0:T(8,128)S(1)} %mul.82, f32[192]{0:T(256)S(1)} %add_rsqrt_fusion, f32[192]{0:T(256)S(1)} %broadcast_multiply_fusion, bf16[192,64,64]{0,2,1:T(8,128)(2,1)S(1)} %bitcast.43), kind=kLoop, calls=%fused_computation.26 | loop fusion | flops 11010048 | bytes 3180032 | tf_op jit(solution)/shard_map/convert_element_type | solution.py:40
  17.8 18.7 %all-to-all-start = ((bf16[192,64,64]{0,2,1:T(8,128)(2,1)}), bf16[192,64,64]{0,2,1:T(8,128)(2,1)S(1)}, u32[]{:S(2)}, u32[]{:S(2)}) async-start(bf16[192,64,64]{0,2,1:T(8,128)(2,1)} %fusion.18), calls=%async_computation | async-start | bytes 4194304 | tf_op jit(solution)/shard_map/all_to_all | solution.py:41
  36.6 0.0 all-gather.5.cloned.1.call-start
  36.6 0.7 all-gather.5.cloned.1.call-update
  37.3 0.2 all-gather.7.cloned.1.call-start
  37.5 33.0 %all-gather.5.cloned.1.call-done = bf16[4,128,1024]{2,1,0:T(8,128)(2,1)} async-done(((bf16[1,128,1024]{2,1,0:T(8,128)(2,1)}), bf16[4,128,1024]{2,1,0:T(8,128)(2,1)}) %all-gather.5.cloned.1.call-update) | async-done | bytes 1048592 | tf_op jit(solution)/shard_map/all_gather | solution.py:22
  70.6 0.0 all-gather.7.cloned.1.call-update
  70.6 25.0 %all-gather.7.cloned.1.call-done = bf16[8,128,1024]{2,1,0:T(8,128)(2,1)} async-done(((bf16[4,128,1024]{2,1,0:T(8,128)(2,1)}), bf16[8,128,1024]{2,1,0:T(8,128)(2,1)}) %all-gather.7.cloned.1.call-update) | async-done | bytes 2097168 | tf_op jit(solution)/shard_map/all_gather | solution.py:22
  95.7 2.2 fusion.19
  97.9 1.5 copy.26
  99.5 37.3 %all-to-all-done = bf16[192,64,64]{0,2,1:T(8,128)(2,1)S(1)} async-done(((bf16[192,64,64]{0,2,1:T(8,128)(2,1)}), bf16[192,64,64]{0,2,1:T(8,128)(2,1)S(1)}, u32[]{:S(2)}, u32[]{:S(2)}) %all-to-all-start) | async-done | bytes 1572896 | tf_op jit(solution)/shard_map/all_to_all | solution.py:41
  136.8 0.0 copy-start.1
  136.8 2.5 copy.25
  139.3 0.0 copy-start
  139.3 5.4 %reshape.112 = bf16[12,1024,64]{1,0,2:T(8,128)(2,1)} reshape(bf16[64,192,64]{1,0,2:T(8,128)(2,1)} %copy.25) | data formatting | bytes 3145728 | tf_op jit(solution)/shard_map/reshape.1
  144.8 0.0 copy-done.1
  144.8 0.0 copy-done
  144.8 3.8 %fusion.33 = bf16[8,8,12,1024]{3,1,0,2:T(8,128)(2,1)S(1)} fusion(f32[1024]{0:T(1024)S(1)} %bitcast.49, bf16[1024,1024,1]{1,0,2:T(8,128)(2,1)S(1)} %bitcast.48, bf16[12,1024,64]{1,0,2:T(8,128)(2,1)} %reshape.112), kind=kOutput, calls=%fused_computation.43 | convolution fusion | flops 1612185600 | bytes 5246976 | tf_op jit(solution)/shard_map/gqp,npgc->nqgc/dot_general | solution.py:50
  148.5 1.3 copy.31
  149.8 3.6 %all_to_all.22 = bf16[64,192,64]{1,0,2:T(8,128)(2,1)S(1)} reshape(bf16[12288,64]{0,1:T(8,128)(2,1)} %bitcast.46) | data formatting | bytes 3145728 | tf_op jit(solution)/shard_map/all_to_all | solution.py:53
  153.4 1.2 copy.29
  154.6 105.4 %all_to_all.26 = bf16[64,192,64]{1,2,0:T(8,128)(2,1)S(1)} all-to-all(bf16[64,192,64]{1,2,0:T(8,128)(2,1)S(1)} %copy.29), channel_id=1, replica_groups=mesh['sp'=64,'dp_0'=4,'dp_1'=2] {'sp'}, dimensions={0} | all-to-all | bytes 3145728 | tf_op jit(solution)/shard_map/all_to_all | solution.py:53
  259.9 2.5 convert_element_type.61
  262.4 3.7 %copy.30 = f32[1,192,4096]{2,1,0:T(8,128)S(1)} copy(f32[1,192,4096]{1,2,0:T(8,128)} %bitcast.44) | data formatting | bytes 6291456 | tf_op jit(solution)/shard_map/convert_element_type | solution.py:55
  266.2 3.7 %fusion.26 = bf16[1,192,4096]{2,1,0:T(8,128)(2,1)} fusion(f32[1,192,4096]{2,1,0:T(8,128)S(1)} %copy.30, bf16[1,192,4096]{2,1,0:T(8,128)(2,1)} %param.6), kind=kLoop, calls=%fused_computation.34 | loop fusion | flops 8650752 | bytes 6291456 | tf_op jit(solution)/shard_map/convert_element_type | solution.py:56
  (3 shorter events, 0.0 us)
Async XLA Ops:
  17.8 119.0 %all-to-all-start = ((bf16[192,64,64]{0,2,1:T(8,128)(2,1)}), bf16[192,64,64]{0,2,1:T(8,128)(2,1)S(1)}, u32[]{:S(2)}, u32[]{:S(2)}) async-start(bf16[192,64,64]{0,2,1:T(8,128)(2,1)} %fusion.18), calls=%async_computation | async-start | bytes 4194304 | tf_op jit(solution)/shard_map/all_to_all | solution.py:41
  36.6 34.0 %all-gather.5.cloned.1.call-start = ((), (), s32[]{:S(2)}) async-start(), calls=%async_computation.2 | async-start | bytes 1310720 | tf_op jit(solution)/shard_map/all_gather | solution.py:22
  37.3 58.4 %all-gather.7.cloned.1.call-start = ((), (), s32[]{:S(2)}) async-start(), calls=%async_computation.3 | async-start | bytes 3145728 | tf_op jit(solution)/shard_map/all_gather | solution.py:22
  136.8 7.9 %copy-start.1 = (f32[1,1024]{1,0:T(1,128)S(1)}, f32[1,1024]{1,0:T(1,128)}, u32[]{:S(2)}) copy-start(f32[1,1024]{1,0:T(1,128)} %param.11) | copy-start | bytes 12292
  139.3 5.4 %copy-start = (bf16[4,2,1,128,1024]{4,3,1,0,2:T(8,128)(2,1)S(1)}, bf16[4,2,1,128,1024]{4,3,1,0,2:T(8,128)(2,1)}, u32[]{:S(2)}) copy-start(bf16[4,2,1,128,1024]{4,3,1,0,2:T(8,128)(2,1)} %copy.26) | copy-start | bytes 6291460
Sparse Core Ops, SparseCore 0:
  39.5 31.0 all-gather.4
  72.7 22.9 all-gather.6
where the time goes:
time: 277 us
  blocking collectives  105 us (38%)
  waiting for transfers between devices  96.1 us (35%)
  local copies, waits for them, and re-layouts  24 us (9%)
  starting transfers between devices  19 us (7%)
  other arithmetic  15.1 us (5%)
  between operations  13.5 us (5%)
  matrix products  3.76 us (1%)
    all_to_all x1, blocking collectives, local(): lax.all_to_all(mixed_flat, 'sp', split_axis=0, concat_axis=1, tiled=True)  105 us
    all_gather x2, waiting for transfers between devices, all_blocks(): parts = lax.all_gather(parts, axes[k], axis=0, tiled=True)  58.1 us
    all_to_all x1, waiting for transfers between devices, local(): lax.all_to_all(normed, 'sp', split_axis=1, concat_axis=0, tiled=True)  37.3 us
    all_to_all x1, starting transfers between devices, local(): lax.all_to_all(normed, 'sp', split_axis=1, concat_axis=0, tiled=True)  18.7 us
  transfers between devices with their start and end apart: 3, of which 3 were waited for; matrix products, arithmetic and copies ran while one was open for 1% of the time, Pallas kernels for 0%

commit v1 on v0

--- a/solution.py
+++ b/solution.py
@@ -3,6 +3,7 @@
 from jax import lax
 from jax.sharding import Mesh
 from jax.sharding import PartitionSpec as P
+from jax.lax import all_to_all, axis_size
 
 GROUP_DIM = 64
 SPAN = 1024
@@ -19,7 +20,8 @@
 def all_blocks(shard, axes, sequence):
     parts = shard[None]
     for k in sequence:
-        parts = lax.all_gather(parts, axes[k], axis=0, tiled=True)
+        obj = axes[k]
+        parts = jnp.concatenate(all_to_all(jnp.stack(axis_size(obj) * [parts], 0), obj, 0, 0), 0)
     current = [lax.axis_size(axes[k]) for k in reversed(sequence)]
     parts = parts.reshape(*current, *shard.shape)
     turned = sorted(range(len(sequence)), key=lambda place: sequence[len(sequence) - 1 - place])

time: 277 us -> 279 us (level)
  the two profiles are of different devices: /device:TPU:2 before, /device:TPU:8 now
where the time goes in v1:
time: 279 us
  blocking collectives  111 us (40%)
  waiting for transfers between devices  103 us (37%)
  starting transfers between devices  23.2 us (8%)
  local copies, waits for them, and re-layouts  21.7 us (8%)
  other arithmetic  15 us (5%)
  matrix products  4.37 us (2%)
    all_to_all x1, blocking collectives, local(): lax.all_to_all(mixed_flat, 'sp', split_axis=0, concat_axis=1, tiled=True)  105 us
    all_to_all x1, waiting for transfers between devices, local(): lax.all_to_all(normed, 'sp', split_axis=1, concat_axis=0, tiled=True)  98.3 us
    all_to_all x1, starting transfers between devices, local(): lax.all_to_all(normed, 'sp', split_axis=1, concat_axis=0, tiled=True)  18.9 us
  transfers between devices with their start and end apart: 2, of which 2 were waited for; matrix products, arithmetic and copies ran while one was open for 4% of the time, Pallas kernels for 0%

profile of v1, /device:TPU:8, one launch (start us, length us, event | category | flops | bytes accessed | tf_op | source)
XLA Modules:
  0.0 278.6 jit_solution(8794174387962564018)
XLA Ops:
  0.0 0.0 copy-start
  0.0 0.0 copy-start.1
  0.0 2.1 stack.6
  2.1 4.3 %all-to-all-start.1 = ((bf16[4,1,1,128,1024]{4,3,2,1,0:T(8,128)(2,1)}), bf16[4,1,1,128,1024]{4,3,2,1,0:T(8,128)(2,1)S(1)}, u32[]{:S(2)}, u32[]{:S(2)}) async-start(bf16[4,1,1,128,1024]{4,3,2,1,0:T(8,128)(2,1)} %stack.6), calls=%async_computation.1 | async-start | bytes 2097152 | tf_op jit(solution)/shard_map/all_to_all | solution.py:24
  6.4 0.0 copy-done
  6.4 0.1 mul.82
  6.4 0.0 copy-done.1
  6.4 0.1 add.70
  6.5 3.1 %copy.29 = bf16[1,192,4096]{1,2,0:T(8,128)(2,1)S(1)} copy(bf16[1,192,4096]{2,1,0:T(8,128)(2,1)} %param.7) | data formatting | bytes 3145728 | tf_op args[1]
  9.7 1.6 fusion.28
  11.3 1.8 multiply_reduce_fusion
  13.1 3.2 %fusion.18 = bf16[192,64,64]{0,2,1:T(8,128)(2,1)} fusion(f32[64,64]{1,0:T(8,128)S(1)} %add.70, f32[64,64]{1,0:T(8,128)S(1)} %mul.82, f32[192]{0:T(256)S(1)} %add_rsqrt_fusion, f32[192]{0:T(256)S(1)} %broadcast_multiply_fusion, bf16[192,64,64]{0,2,1:T(8,128)(2,1)S(1)} %bitcast.44), kind=kLoop, calls=%fused_computation.26 | loop fusion | flops 11010048 | bytes 3180032 | tf_op jit(solution)/shard_map/convert_element_type | solution.py:42
  16.3 5.2 %all-to-all-done.1 = bf16[4,1,1,128,1024]{4,3,2,1,0:T(8,128)(2,1)S(1)} async-done(((bf16[4,1,1,128,1024]{4,3,2,1,0:T(8,128)(2,1)}), bf16[4,1,1,128,1024]{4,3,2,1,0:T(8,128)(2,1)S(1)}, u32[]{:S(2)}, u32[]{:S(2)}) %all-to-all-start.1) | async-done | bytes 1048608 | tf_op jit(solution)/shard_map/all_to_all | solution.py:24
  21.5 0.2 pad_maximum_fusion
  21.6 5.4 %all_to_all.36 = bf16[2,4,1,128,1024]{4,3,1,2,0:T(8,128)(2,1)S(1)} all-to-all(bf16[2,4,1,128,1024]{4,3,1,2,0:T(8,128)(2,1)S(1)} %pad_maximum_fusion), channel_id=1, replica_groups=mesh['sp'=64,'dp_0'=4,'dp_1'=2] {'dp_1'}, dimensions={0} | all-to-all | bytes 4194304 | tf_op jit(solution)/shard_map/all_to_all | solution.py:24
  27.1 18.9 %all-to-all-start = ((bf16[192,64,64]{0,2,1:T(8,128)(2,1)}), bf16[192,64,64]{0,2,1:T(8,128)(2,1)}, u32[]{:S(2)}, u32[]{:S(2)}) async-start(bf16[192,64,64]{0,2,1:T(8,128)(2,1)} %fusion.18), calls=%async_computation | async-start | bytes 4194304 | tf_op jit(solution)/shard_map/all_to_all | solution.py:43
  46.0 2.0 fusion.19
  48.0 98.3 %all-to-all-done = bf16[192,64,64]{0,2,1:T(8,128)(2,1)} async-done(((bf16[192,64,64]{0,2,1:T(8,128)(2,1)}), bf16[192,64,64]{0,2,1:T(8,128)(2,1)}, u32[]{:S(2)}, u32[]{:S(2)}) %all-to-all-start) | async-done | bytes 1572896 | tf_op jit(solution)/shard_map/all_to_all | solution.py:43
  146.3 2.8 copy.30
  149.1 0.0 copy-start.2
  149.1 3.8 %reshape.112 = bf16[12,1024,64]{1,0,2:T(8,128)(2,1)} reshape(bf16[64,192,64]{1,0,2:T(8,128)(2,1)S(1)} %copy.30) | data formatting | bytes 3145728 | tf_op jit(solution)/shard_map/reshape.2
  152.9 0.0 copy-done.2
  152.9 4.4 %fusion.33 = bf16[8,8,12,1024]{3,1,0,2:T(8,128)(2,1)S(1)} fusion(f32[1024]{0:T(1024)S(1)} %bitcast.50, bf16[1024,1024,1]{1,0,2:T(8,128)(2,1)} %bitcast.48, bf16[12,1024,64]{1,0,2:T(8,128)(2,1)} %reshape.112), kind=kOutput, calls=%fused_computation.44 | convolution fusion | flops 1612185600 | bytes 5246976 | tf_op jit(solution)/shard_map/gqp,npgc->nqgc/dot_general | solution.py:52
  157.3 1.3 copy.36
  158.6 3.6 %all_to_all.30 = bf16[64,192,64]{1,0,2:T(8,128)(2,1)S(1)} reshape(bf16[12288,64]{0,1:T(8,128)(2,1)} %bitcast.46) | data formatting | bytes 3145728 | tf_op jit(solution)/shard_map/all_to_all | solution.py:55
  162.2 1.2 copy.34
  163.3 105.3 %all_to_all.37 = bf16[64,192,64]{1,2,0:T(8,128)(2,1)S(1)} all-to-all(bf16[64,192,64]{1,2,0:T(8,128)(2,1)S(1)} %copy.34), channel_id=1, replica_groups=mesh['sp'=64,'dp_0'=4,'dp_1'=2] {'sp'}, dimensions={0} | all-to-all | bytes 3145728 | tf_op jit(solution)/shard_map/all_to_all | solution.py:55
  268.7 2.5 convert_element_type.61
  271.2 3.7 %copy.35 = f32[1,192,4096]{2,1,0:T(8,128)S(1)} copy(f32[1,192,4096]{1,2,0:T(8,128)} %bitcast.45) | data formatting | bytes 6291456 | tf_op jit(solution)/shard_map/convert_element_type | solution.py:57
  274.9 3.7 %fusion.26 = bf16[1,192,4096]{2,1,0:T(8,128)(2,1)} fusion(f32[1,192,4096]{2,1,0:T(8,128)S(1)} %copy.35, bf16[1,192,4096]{2,1,0:T(8,128)(2,1)} %param.6), kind=kLoop, calls=%fused_computation.34 | loop fusion | flops 8650752 | bytes 6291456 | tf_op jit(solution)/shard_map/convert_element_type | solution.py:58
  (3 shorter events, 0.0 us)
Async XLA Ops:
  0.0 6.4 %copy-start = (f32[4096]{0:T(1024)S(1)}, f32[4096]{0:T(1024)}, u32[]{:S(2)}) copy-start(f32[4096]{0:T(1024)} %param.8) | copy-start | bytes 49156
  0.0 6.4 %copy-start.1 = (f32[4096]{0:T(1024)S(1)}, f32[4096]{0:T(1024)}, u32[]{:S(2)}) copy-start(f32[4096]{0:T(1024)} %param.9) | copy-start | bytes 49156
  2.1 19.4 %all-to-all-start.1 = ((bf16[4,1,1,128,1024]{4,3,2,1,0:T(8,128)(2,1)}), bf16[4,1,1,128,1024]{4,3,2,1,0:T(8,128)(2,1)S(1)}, u32[]{:S(2)}, u32[]{:S(2)}) async-start(bf16[4,1,1,128,1024]{4,3,2,1,0:T(8,128)(2,1)} %stack.6), calls=%async_computation.1 | async-start | bytes 2097152 | tf_op jit(solution)/shard_map/all_to_all | solution.py:24
  27.1 119.3 %all-to-all-start = ((bf16[192,64,64]{0,2,1:T(8,128)(2,1)}), bf16[192,64,64]{0,2,1:T(8,128)(2,1)}, u32[]{:S(2)}, u32[]{:S(2)}) async-start(bf16[192,64,64]{0,2,1:T(8,128)(2,1)} %fusion.18), calls=%async_computation | async-start | bytes 4194304 | tf_op jit(solution)/shard_map/all_to_all | solution.py:43
  149.1 3.8 %copy-start.2 = (f32[1,1024]{1,0:T(1,128)S(1)}, f32[1,1024]{1,0:T(1,128)}, u32[]{:S(2)}) copy-start(f32[1,1024]{1,0:T(1,128)} %param.11) | copy-start | bytes 12292
